TPU v7x, 256 devices: a whole 4x4x8 slice. The times are simulated.
256 devices in a mesh: kv: 32 (over z, y), tp: 8 (over x, core).
Axes of the slice: x: 4, y: 4, z: 8, core: 2. Of those that a mesh axis runs over, the one named last changes fastest.
Arguments:
- tokens: bfloat16 [128, 4096], P(None, ('kv', 'tp')), may hold values from -12 to 12
- first_gain: bfloat16 [4096], replicated, may hold values from 0.099609375 to 1.8984375
- first_gate: bfloat16 [4096, 11264], P(None, ('kv', 'tp')), may hold values from -0.09375 to 0.09375
- first_up: bfloat16 [4096, 11264], P(None, ('kv', 'tp')), may hold values from -0.09375 to 0.09375
- first_down: bfloat16 [11264, 4096], P(('kv', 'tp')), may hold values from -0.25 to 0.25
- mix_gain: bfloat16 [4096], replicated, may hold values from 0.099609375 to 1.8984375
- query_weight: bfloat16 [4096, 1024], P('kv', 'tp'), may hold values from -0.09375 to 0.09375
- key_weight: bfloat16 [4096, 1024], P('kv', 'tp'), may hold values from -0.09375 to 0.09375
- value_weight: bfloat16 [4096, 2048], P('kv', 'tp'), may hold values from -0.09375 to 0.09375
- outgate_weight: bfloat16 [4096, 2048], P('kv', 'tp'), may hold values from -0.09375 to 0.09375
- ingate_weight: bfloat16 [4096, 8], P('kv'), may hold values from -0.09375 to 0.09375
- forget_weight: bfloat16 [4096, 8], P('kv'), may hold values from -0.09375 to 0.09375
- forget_bias: float32 [8], P('tp'), may hold values from -1 to 4
- head_gain: bfloat16 [2048], P('tp'), may hold values from 0.099609375 to 1.8984375
- mixout_weight: bfloat16 [2048, 4096], P('tp', 'kv'), may hold values from -0.125 to 0.125
- memory: float32 [128, 8, 128, 256], P('kv', 'tp'), may hold values from -0.6 to 0.6
- stabilizer: float32 [128, 8], P('kv', 'tp'), may hold values from -4 to 4
- second_gain: bfloat16 [4096], replicated, may hold values from 0.099609375 to 1.8984375
- second_gate: bfloat16 [4096, 11264], P(None, ('kv', 'tp')), may hold values from -0.09375 to 0.09375
- second_up: bfloat16 [4096, 11264], P(None, ('kv', 'tp')), may hold values from -0.09375 to 0.09375
- second_down: bfloat16 [11264, 4096], P(('kv', 'tp')), may hold values from -0.25 to 0.25
Outputs:
- layer_out: bfloat16 [128, 4096], P(None, ('kv', 'tp'))
- memory_next: float32 [128, 8, 128, 256], P('kv', 'tp')
- stabilizer_next: float32 [128, 8], P('kv', 'tp')
All inputs are finite; a program needn't handle non-finite values.
Results may differ from a plain program's by a relative error of at most 0.013.
Values may be sent and summed in bfloat16 or wider, within the bound.
A program may use at most 64 MiB of HBM per device.

v0:
```python
import functools

import jax
import jax.numpy as jnp
from jax import lax
from jax.experimental import pallas as pl
from jax.experimental.pallas import tpu as pltpu
from jax.sharding import PartitionSpec as P

EPS = 1e-06
Y = 4
C = 2
ROWS = 16
SEQ = 4
MESH = pl.DeviceIdType.MESH
bf16 = jnp.bfloat16
f32 = jnp.float32


def nothing():
    pass


def near_first(n):
    return sorted(range(n), key=lambda i: (min(i, n - i), i))


def hops(d, n):
    return min(d, n - d)


def remote(src, dst, send, recv, kv, tp):
    return pltpu.make_async_remote_copy(
        src_ref=src, dst_ref=dst, send_sem=send, recv_sem=recv, device_id=(kv, tp), device_id_type=MESH
    )


def wait_for(ref, sem):
    pltpu.make_async_copy(ref, ref, sem).wait()


def kernel(kv_size, tp_size, *refs):
    Z, X = kv_size // Y, tp_size // C
    YX, TP, B = Y * X, tp_size, SEQ * kv_size
    G = YX * C * ROWS
    D = Z * G
    FK = TP * ROWS
    near, far = near_first(Z), near_first(Z)[::-1]
    plane_far = sorted(range(1, YX), key=lambda p: -hops(p // X, Y) - hops(p % X, X))
    kv_far = sorted(range(1, kv_size), key=lambda p: -hops(p // Y, Z) - hops(p % Y, Y))

    args = (
        "tok", "g1", "wg1", "wu1", "wd1", "gm", "wq", "wk", "wv", "wo", "wi", "wf", "fb", "hg", "wm",
        "mem", "stab", "g2", "wg2", "wu2", "wd2",
    )
    names = args + ("out_o", "mem_o", "stab_o") + tuple(a + "_v" for a in args)
    names += ("gm32", "wmisc", "wmt", "tr", "hid")
    for k in "12":
        names += tuple(
            n + k
            for n in (
                "wgs", "wus", "wds", "wp", "dt", "xall", "ebuf", "erec", "sbuf", "prow", "zbuf", "zrec",
                "sw", "ssw", "az", "saz", "ap", "sap", "ex", "rp", "srp", "rz", "srz",
            )
        )
    names += ("fbuf", "sm", "yrec", "zb", "zr", "mm", "obuf", "of32", "orec", "lsem")
    names += ("fs", "my", "smy", "mz", "smz", "ns", "os")
    r = dict(zip(names, refs, strict=True))

    kv, tp = lax.axis_index("kv"), lax.axis_index("tp")
    z, y = kv // Y, kv % Y
    x, c = tp // C, tp % C
    yx = y * X + x
    other = 1 - c

    barrier = pltpu.get_barrier_semaphore()

    def greet(kv_to, tp_to):
        pl.semaphore_signal(barrier, inc=1, device_id=(kv_to, tp_to), device_id_type=MESH)

    for dz in range(1, Z):
        greet((z + dz) % Z * Y + y, tp)
    for p in range(1, YX):
        greet(z * Y + (y + p // X) % Y, (x + p % X) % X * C + c)
    for dx in range(X):
        greet(kv, (x + dx) % X * C + other)
    for p in kv_far:
        if p // Y and p % Y:
            greet((z + p // Y) % Z * Y + (y + p % Y) % Y, tp)

    copies = {
        n: pltpu.make_async_copy(r[n], r[n + "_v"], r["lsem"].at[i]) for i, n in enumerate(args)
    }
    for n in args:
        copies[n].start()

    for k in "12":
        r["xall" + k][:, :, other] = jnp.zeros((Z, YX, ROWS, B), bf16)
    r["hid"][...] = jnp.zeros_like(r["hid"])
    r["tr"][...] = jnp.zeros_like(r["tr"])
    r["wmisc"][...] = jnp.zeros_like(r["wmisc"])
    copies["tok"].wait()
    pl.semaphore_wait(barrier, (Z - 1) + (YX - 1) + X + (Z - 1) * (Y - 1))

    def plane(send):
        for p in plane_far:
            yt, xt = (y + p // X) % Y, (x + p % X) % X
            send(p, yt * X + xt, z * Y + yt, xt * C + c)

    def swap_weights(k):
        for i, n in enumerate(("wg", "wu", "wd")):
            copies[n + k].wait()
            remote(
                r[n + k + "_v"], r[n + "s" + k], r["ssw" + k].at[i], r["sw" + k].at[i], kv, x * C + other
            ).start()

    def prep_up(k):
        copies["g" + k].wait()
        for i, n in enumerate(("wgs", "wus")):
            wait_for(r[n + k], r["sw" + k].at[i])
        gain, wp = r[f"g{k}_v"][...].astype(f32).reshape(1, D), r["wp" + k]
        for j, n in enumerate((f"wg{k}_v", f"wu{k}_v", "wgs" + k, "wus" + k)):
            for zz in range(Z):
                cols = slice(zz * G, zz * G + G)
                wp[zz, 48 * j + 40 : 48 * j + 48, :] = jnp.zeros((8, G), bf16)
                wp[zz, 48 * j : 48 * j + 44, :] = (r[n][:, cols].astype(f32) * gain[:, cols]).astype(bf16)

    def prep_down(k):
        wait_for(r["wds" + k], r["sw" + k].at[2])
        tr, dt = r["tr"], r["dt" + k]
        for zz in range(Z):
            cols = slice(zz * G, zz * G + G)
            tr[0:44, :] = r[f"wd{k}_v"][:, cols].astype(f32)
            tr[48:92, :] = r["wds" + k][:, cols].astype(f32)
            dt[zz] = jnp.transpose(tr[...]).astype(bf16).reshape(YX, C, ROWS, 128)

    def mlp(k, after_sends, after_z, after_scatter):
        xall, ebuf, erec, sbuf, prow, zbuf, zrec = (
            r[n + k] for n in ("xall", "ebuf", "erec", "sbuf", "prow", "zbuf", "zrec")
        )
        az, ap, ex, rp, rz, saz, sap, srp, srz = (
            r[n + k] for n in ("az", "ap", "ex", "rp", "rz", "saz", "sap", "srp", "srz")
        )
        hid = r["hid"]

        def spread(i):
            def send(p, target, kv_to, tp_to):
                remote(xall.at[i, yx, c], xall.at[i, yx, c], sap.at[i], ap.at[i], kv_to, tp_to).start()

            plane(send)

        for dz in far:
            if dz:
                kv_to = (z + dz) % Z * Y + y
                remote(xall.at[0, yx, c], xall.at[dz, yx, c], saz.at[dz], az.at[dz], kv_to, tp).start()
        spread(0)
        after_sends()
        for i in near[1:]:
            wait_for(xall.at[i, yx, c], az.at[i])
            spread(i)
        after_z()

        squares = jnp.zeros((8, B), f32)
        sums = jnp.zeros((192, B), f32)
        for i in near:
            wait_for(prow.at[0, pl.ds(1, YX - 1)], ap.at[i])
            sums += jnp.dot(
                r["wp" + k][(z - i + Z) % Z], xall[i].reshape(G, B), preferred_element_type=f32
            )
            wide = xall[i, :, c].astype(f32)
            squares += jnp.sum((wide * wide).reshape(YX * ROWS // 8, 8, B), axis=0)
        ebuf[0:192] = sums
        ebuf[192:200] = squares
        both = remote(ebuf, erec, ex.at[0], ex.at[1], kv, x * C + other)
        both.start()
        both.wait_recv()
        squares = ebuf[192:200] + erec[192:200]
        factor = lax.rsqrt(jnp.sum(squares, axis=0, keepdims=True) / D + EPS)
        for mine, theirs in ((0, 96), (96, 0)):
            total = factor * (ebuf[mine : mine + 96] + erec[theirs : theirs + 96])
            gate, up = total[0:48], total[48:96]
            hid[mine // 2 : mine // 2 + 48] = (gate / (1.0 + jnp.exp(-gate)) * up).astype(bf16)

        for i in far:
            weight = r["dt" + k][(z + i) % Z, :, c].reshape(YX * ROWS, 128)
            terms = jnp.dot(weight, hid[...], preferred_element_type=f32)
            sbuf[i] = terms.reshape(YX, ROWS, B).astype(bf16)

            def send(p, target, kv_to, tp_to):
                remote(sbuf.at[i, target], prow.at[i, p], srp.at[i], rp.at[i], kv_to, tp_to).start()

            plane(send)
        after_scatter()

        total = None
        for i in far:
            wait_for(prow.at[i, pl.ds(1, YX - 1)], rp.at[i])
            total = jnp.sum(prow[i, 1:YX].astype(f32), axis=0) + sbuf[i, yx].astype(f32)
            if i:
                zbuf[i] = total
                kv_to = (z + i) % Z * Y + y
                remote(zbuf.at[i], zrec.at[i], srz.at[i], rz.at[i], kv_to, tp).start()
        for i in near[1:]:
            wait_for(zrec.at[i], rz.at[i])
            total = total + zrec[i]

        def drain():
            both.wait_send()
            for i, n in enumerate(("wgs", "wus", "wds")):
                wait_for(r[n + k], r["ssw" + k].at[i])
            for i in range(Z):
                if i:
                    wait_for(xall.at[0, yx, c], saz.at[i])
                    wait_for(zbuf.at[i], srz.at[i])
                wait_for(prow.at[i, pl.ds(1, YX - 1)], sap.at[i])
                wait_for(prow.at[i, pl.ds(1, YX - 1)], srp.at[i])

        return 0.5 * total, drain

    r["xall1"][0, yx, c] = r["tok_v"][...]

    def prep_mix():
        for n in ("gm", "wq", "wk", "wv", "wo", "wi", "wf", "fb", "hg", "wm", "mem", "stab"):
            copies[n].wait()
        heads = r["wi_v"].shape[0]
        r["wmisc"][0, 0:heads] = r["wi_v"][...]
        r["wmisc"][1, 0:heads] = r["wf_v"][...]
        r["gm32"][...] = r["gm_v"][...].astype(f32).reshape(1, D)
        r["wmt"][...] = jnp.transpose(r["wm_v"][...].astype(f32)).astype(bf16)

    def prep_first():
        prep_up("1")
        prep_down("1")

    def prep_second():
        swap_weights("2")
        prep_mix()
        prep_up("2")
        prep_down("2")

    half, drain1 = mlp("1", lambda: swap_weights("1"), prep_first, prep_second)
    first = (r["tok_v"][...].astype(f32) + half).astype(bf16)

    fbuf = r["fbuf"]
    fbuf[tp] = first
    for d in range(1, TP):
        remote(fbuf.at[tp], fbuf.at[tp], r["fs"].at[0], r["fs"].at[1], kv, (tp + d) % TP).start()
    wait_for(fbuf.at[pl.ds(1, TP - 1)], r["fs"].at[1])
    wide = jnp.transpose(fbuf[...].reshape(FK, B).astype(f32))
    row_squares = jnp.sum(wide * wide, axis=1, keepdims=True)
    gain = r["gm32"][:, pl.ds(pl.multiple_of(kv * FK, FK), FK)]
    w = (wide * gain).astype(bf16)

    def project(matrix):
        return jnp.dot(w, matrix, preferred_element_type=f32)

    def project_rows(matrix):
        return lax.dot_general(w, matrix, (((1,), (1,)), ((), ())), preferred_element_type=f32)

    lane = lax.broadcasted_iota(jnp.int32, (B, 128), 1)
    pieces = (
        project(r["wq_v"][...]),
        project(r["wk_v"][...]),
        project(r["wv_v"][:, 0:128]),
        project(r["wv_v"][:, 128:256]),
        project(r["wo_v"][:, 0:128]),
        project(r["wo_v"][:, 128:256]),
        jnp.where(lane == 8, row_squares, project_rows(r["wmisc"][0])),
        project_rows(r["wmisc"][1]),
    )
    sm = r["sm"]
    low = lax.broadcasted_iota(jnp.int32, (B // 8, 8, 128), 1) < 4
    for m in range(4):
        even, odd = (p.reshape(B // 8, 8, 128) for p in pieces[2 * m : 2 * m + 2])
        sm[:, 0, 8 * m : 8 * m + 8] = jnp.where(low, even, pltpu.roll(odd, 4, 1)).astype(bf16)
        sm[:, 1, 8 * m : 8 * m + 8] = jnp.where(low, pltpu.roll(even, 4, 1), odd).astype(bf16)

    yrec, zb, zr = r["yrec"], r["zb"], r["zr"]

    def seqs(kv_of):
        return kv_of // 2, kv_of % 2

    for i in far:
        zt = (z + i) % Z
        for dy in range(1, Y):
            a, b = seqs(zt * Y + (y + dy) % Y)
            remote(
                sm.at[a, b], yrec.at[i, dy], r["smy"].at[i], r["my"].at[i], z * Y + (y + dy) % Y, tp
            ).start()
    mine = None
    for i in far:
        wait_for(yrec.at[i, pl.ds(1, Y - 1)], r["my"].at[i])
        a, b = seqs((z + i) % Z * Y + y)
        mine = jnp.sum(yrec[i, 1:Y].astype(f32), axis=0) + sm[a, b].astype(f32)
        if i:
            zb[i] = mine.astype(bf16)
            remote(zb.at[i], zr.at[i], r["smz"].at[i], r["mz"].at[i], (z + i) % Z * Y + y, tp).start()
    for i in near[1:]:
        wait_for(zr.at[i], r["mz"].at[i])
        mine = mine + zr[i].astype(f32)

    lane8 = lax.broadcasted_iota(jnp.int32, (8, 128), 1)
    row8 = lax.broadcasted_iota(jnp.int32, (8, 128), 0)
    top = row8 < 4

    def rounded(v):
        return v.astype(bf16).astype(f32)

    def pick(v, at):
        return jnp.broadcast_to(jnp.sum(jnp.where(lane8 == at, v, 0.0), axis=1, keepdims=True), (8, 128))

    def both(v):
        return v + pltpu.roll(v, 4, 0)

    misc = mine[24:32]
    factor = lax.rsqrt(both(jnp.where(top, pick(misc, 8), 0.0)) / D + EPS)
    gates = pick(misc, tp) * factor
    ingate = jnp.where(top, gates, pltpu.roll(gates, 4, 0))
    forget = jnp.where(top, pltpu.roll(gates, 4, 0), gates) + r["fb_v"][...]
    spread4 = lax.broadcasted_iota(jnp.int32, (8, SEQ), 0) % SEQ == lax.broadcasted_iota(jnp.int32, (8, SEQ), 1)
    stab = jnp.sum(jnp.where(spread4, r["stab_v"][...], 0.0), axis=1, keepdims=True)
    log_forget = jnp.minimum(forget, 0.0) - jnp.log1p(jnp.exp(-jnp.abs(forget)))
    carried = log_forget + stab
    ceiling = jnp.maximum(carried, ingate)
    retain, admit = jnp.exp(carried - ceiling), jnp.exp(ingate - ceiling)
    diagonal = (row8 == lane8) & top
    r["stab_o"][...] = jnp.sum(jnp.where(diagonal, ceiling, 0.0), axis=0, keepdims=True)[:, 0:SEQ]

    qk = rounded(factor * mine[0:8])
    values = rounded(factor * mine[8:16])
    outgate = rounded(factor * mine[16:24])
    qk_cols = jnp.transpose(qk)
    scaled = 128**-0.5
    readout = jnp.zeros((8, 128), f32)
    for s in range(SEQ):
        q_col = jnp.broadcast_to(qk_cols[:, s : s + 1], (128, 128))
        k_col = jnp.broadcast_to(qk_cols[:, 4 + s : 5 + s] * scaled, (128, 128))
        for h in range(2):
            at = 4 * h + s
            old = r["mem_v"][s, 0, :, 128 * h : 128 * h + 128]
            new = retain[s : s + 1] * old + admit[s : s + 1] * (k_col * values[at : at + 1])
            r["mem_o"][s, 0, :, 128 * h : 128 * h + 128] = new
            readout = jnp.where(row8 == at, jnp.sum(q_col * new, axis=0, keepdims=True), readout)
    mean = both(jnp.broadcast_to(jnp.sum(readout * readout, axis=1, keepdims=True), (8, 128))) / 256
    hg = r["hg_v"]
    hg = hg[...].astype(f32).reshape(1, 256)
    head_gain = jnp.where(top, hg[:, 0:128], hg[:, 128:256])
    gated = readout * lax.rsqrt(mean + EPS) * head_gain / (1.0 + jnp.exp(-outgate))

    mm = r["mm"]
    mm[kv] = rounded(gated)
    for p in kv_far:
        kv_to = (z + p // Y) % Z * Y + (y + p % Y) % Y
        remote(mm.at[kv], mm.at[kv], r["ns"].at[0], r["ns"].at[1], kv_to, tp).start()
    others = mm.at[pl.ds(0, kv_size - 1)]
    wait_for(others, r["ns"].at[1])
    pairs = mm[...].reshape(B // 8, 2, 8, 128)
    a, b = pairs[:, 0], pairs[:, 1]
    left = jnp.where(low, a, pltpu.roll(b, 4, 1)).reshape(B, 128).astype(bf16)
    right = jnp.where(low, pltpu.roll(a, 4, 1), b).reshape(B, 128).astype(bf16)

    def across(m, v):
        return lax.dot_general(m, v, (((1,), (1,)), ((), ())), preferred_element_type=f32)

    terms = across(r["wmt"][:, 0:128], left) + across(r["wmt"][:, 128:256], right)
    terms = terms.reshape(TP, ROWS, B)
    r["of32"][...] = terms
    r["obuf"][...] = terms.astype(bf16)
    for d in range(1, TP):
        to = (tp + d) % TP
        remote(r["obuf"].at[to], r["orec"].at[d], r["os"].at[0], r["os"].at[1], kv, to).start()
    wait_for(r["orec"].at[pl.ds(1, TP - 1)], r["os"].at[1])
    branch = r["of32"][tp] + jnp.sum(r["orec"][1:TP].astype(f32), axis=0)
    after_mix = (first.astype(f32) + branch).astype(bf16)

    r["xall2"][0, yx, c] = after_mix
    half, drain2 = mlp("2", nothing, nothing, nothing)
    r["out_o"][...] = (after_mix.astype(f32) + half).astype(bf16)
    drain1()
    drain2()
    wait_for(fbuf.at[pl.ds(1, TP - 1)], r["fs"].at[0])
    wait_for(r["orec"].at[pl.ds(1, TP - 1)], r["os"].at[0])
    wait_for(others, r["ns"].at[0])
    for i in range(Z):
        wait_for(yrec.at[i, pl.ds(1, Y - 1)], r["smy"].at[i])
        if i:
            wait_for(zb.at[i], r["smz"].at[i])


def on_device(kv_size, tp_size, *args):
    (
        tokens, first_gain, first_gate, first_up, first_down, mix_gain,
        query_weight, key_weight, value_weight, outgate_weight, ingate_weight, forget_weight,
        forget_bias, head_gain, mixout_weight, memory, stabilizer,
        second_gain, second_gate, second_up, second_down,
    ) = args
    operands = (
        tokens.T, first_gain, first_gate.T, first_up.T, first_down, mix_gain,
        query_weight, key_weight, value_weight, outgate_weight, ingate_weight.T, forget_weight.T,
        forget_bias[None], head_gain, mixout_weight, memory, stabilizer.T,
        second_gain, second_gate.T, second_up.T, second_down,
    )
    Z, X = kv_size // Y, tp_size // C
    YX, TP, B = Y * X, tp_size, SEQ * kv_size
    G = YX * C * ROWS
    out_shapes = (
        jax.ShapeDtypeStruct((ROWS, B), bf16),
        jax.ShapeDtypeStruct(memory.shape, f32),
        jax.ShapeDtypeStruct((1, SEQ), f32),
    )
    DMA = pltpu.SemaphoreType.DMA
    raw = pltpu.VMEM(first_down.shape, bf16)
    block = (
        raw,
        raw,
        raw,
        pltpu.VMEM((Z, 192, G), bf16),
        pltpu.VMEM((Z, YX, C, ROWS, 128), bf16),
        pltpu.VMEM((Z, YX, C, ROWS, B), bf16),
        pltpu.VMEM((200, B), f32),
        pltpu.VMEM((200, B), f32),
        pltpu.VMEM((Z, YX, ROWS, B), bf16),
        pltpu.VMEM((Z, YX, ROWS, B), bf16),
        pltpu.VMEM((Z, ROWS, B), f32),
        pltpu.VMEM((Z, ROWS, B), f32),
        DMA((3,)),
        DMA((3,)),
        DMA((Z,)),
        DMA((Z,)),
        DMA((Z,)),
        DMA((Z,)),
        DMA((2,)),
        DMA((Z,)),
        DMA((Z,)),
        DMA((Z,)),
        DMA((Z,)),
    )
    scratch = (
        *(pltpu.VMEM(o.shape, o.dtype) for o in operands),
        pltpu.VMEM((1, mix_gain.shape[0]), f32),
        pltpu.VMEM((2, 128, TP * ROWS), bf16),
        pltpu.VMEM((TP * ROWS, 256), bf16),
        pltpu.VMEM((128, G), f32),
        pltpu.VMEM((128, B), bf16),
        *block,
        *block,
        pltpu.VMEM((TP, ROWS, B), bf16),
        pltpu.VMEM((kv_size // 2, 2, 32, 128), bf16),
        pltpu.VMEM((Z, Y, 32, 128), bf16),
        pltpu.VMEM((Z, 32, 128), bf16),
        pltpu.VMEM((Z, 32, 128), bf16),
        pltpu.VMEM((kv_size, 8, 128), f32),
        pltpu.VMEM((TP, ROWS, B), bf16),
        pltpu.VMEM((TP, ROWS, B), f32),
        pltpu.VMEM((TP, ROWS, B), bf16),
        DMA((len(operands),)),
        DMA((2,)),
        DMA((Z,)),
        DMA((Z,)),
        DMA((Z,)),
        DMA((Z,)),
        DMA((2,)),
        DMA((2,)),
    )
    out, memory_next, stabilizer_next = pl.pallas_call(
        functools.partial(kernel, kv_size, tp_size),
        out_shape=out_shapes,
        in_specs=[pl.BlockSpec(memory_space=pl.ANY)] * len(operands),
        out_specs=[pl.BlockSpec(memory_space=pltpu.VMEM)] * 3,
        scratch_shapes=scratch,
        compiler_params=pltpu.CompilerParams(
            collective_id=0, has_side_effects=True, vmem_limit_bytes=60 * 1024 * 1024
        ),
        name="decode_step",
    )(*operands)
    return out.T, memory_next, stabilizer_next.T


def solution(mesh):
    in_specs = (
        P(None, ("kv", "tp")),
        P(),
        P(None, ("kv", "tp")),
        P(None, ("kv", "tp")),
        P(("kv", "tp"), None),
        P(),
        P("kv", "tp"),
        P("kv", "tp"),
        P("kv", "tp"),
        P("kv", "tp"),
        P("kv", None),
        P("kv", None),
        P("tp"),
        P("tp"),
        P("tp", "kv"),
        P("kv", "tp", None, None),
        P("kv", "tp"),
        P(),
        P(None, ("kv", "tp")),
        P(None, ("kv", "tp")),
        P(("kv", "tp"), None),
    )
    out_specs = (P(None, ("kv", "tp")), P("kv", "tp", None, None), P("kv", "tp"))
    return jax.shard_map(
        functools.partial(on_device, mesh.shape["kv"], mesh.shape["tp"]),
        mesh=mesh,
        in_specs=in_specs,
        out_specs=out_specs,
        check_vma=False,
    )
```

profile of v0, /device:TPU:1, one launch (start us, length us, event | category | flops | bytes accessed | tf_op | source)
XLA Modules:
  0.0 87.0 jit_solution(6478874686612861558)
XLA Ops:
  1.3 82.1 %decode_step.1 = (bf16[16,128]{1,0:T(8,128)(2,1)}, f32[4,1,128,256]{3,2,1,0:T(8,128)}, f32[1,4]{1,0:T(1,128)}) custom-call(bf16[16,128]{1,0:T(8,128)(2,1)} %bitcast.16, bf16[4096]{0:T(1024)(128)(2,1)} %refs_1_.1, bf16[44,4096]{1,0:T(8,128)(2,1)} %bitcast.12, bf16[44,4096]{1,0:T(8,128)(2,1)} %bitcast.13, bf16[44,4096]{1,0:T(8,128)(2,1)} %refs_4_.1, ...), custom_call_target="tpu_custom_call" | custom-call | tf_op jit(solution)/shard_map/decode_step/pallas_call | solution.py:465
  83.4 0.0 copy-start
  83.4 0.7 copy-done
  84.0 0.6 copy.28
  84.6 0.0 copy-start.1
  84.6 1.9 %copy.29 = f32[4,1,128,256]{3,2,1,0:T(8,128)} copy(f32[4,1,128,256]{3,2,1,0:T(8,128)} %get-tuple-element.13) | data formatting | bytes 1048576
  86.5 0.0 copy-done.1
  86.5 0.5 copy.30
Async XLA Ops:
  83.4 0.7 copy-start
  84.6 1.9 %copy-start.1 = (f32[1,4]{1,0:T(1,128)S(1)}, f32[1,4]{1,0:T(1,128)}, u32[]{:S(2)}) copy-start(f32[1,4]{1,0:T(1,128)} %get-tuple-element.8) | copy-start | bytes 52
where the time goes:
time: 87.2 us; the launch traced here: 87 us
  Pallas kernels  82.1 us (94%)
  local copies, waits for them, and re-layouts  3.64 us (4%)
  between operations  1.3 us (1%)
    pallas_call x1, Pallas kernels, on_device(): pl.pallas_call(functools.partial(kernel, kv_size, tp_size), out_shape=out...  82.1 us
    unnamed x7, local copies, waits for them, and re-layouts  3.64 us

commit v1 on v0

--- a/solution.py
+++ b/solution.py
@@ -12,6 +12,14 @@
 C = 2
 ROWS = 16
 SEQ = 4
+AG_GROUPS = ((0,), (3, 4), (5, 6, 7))
+AG_DIRECT = (1, 2)
+AG_ORDER = ((0,), (1,), (2,), (3, 4), (5, 6, 7))
+RS_ORDER = ((1,), (2,), (7,), (5,), (6,), (3,), (4,), (0,))
+RS_DIRECT = ()
+RS_FIRST = (1, 2)
+AG_LATE = ()
+KS_DIRECT = (5, 6, 7)
 MESH = pl.DeviceIdType.MESH
 bf16 = jnp.bfloat16
 f32 = jnp.float32
@@ -59,7 +67,7 @@
         names += tuple(
             n + k
             for n in (
-                "wgs", "wus", "wds", "wp", "dt", "xall", "ebuf", "erec", "sbuf", "prow", "zbuf", "zrec",
+                "wgs", "wus", "wds", "wp", "dt", "xall", "ebuf", "erec", "sbuf", "prow", "drow", "first", "zbuf", "zrec",
                 "sw", "ssw", "az", "saz", "ap", "sap", "ex", "rp", "srp", "rz", "srz",
             )
         )
@@ -73,39 +81,39 @@
     yx = y * X + x
     other = 1 - c
 
-    barrier = pltpu.get_barrier_semaphore()
-
-    def greet(kv_to, tp_to):
-        pl.semaphore_signal(barrier, inc=1, device_id=(kv_to, tp_to), device_id_type=MESH)
-
-    for dz in range(1, Z):
-        greet((z + dz) % Z * Y + y, tp)
-    for p in range(1, YX):
-        greet(z * Y + (y + p // X) % Y, (x + p % X) % X * C + c)
-    for dx in range(X):
-        greet(kv, (x + dx) % X * C + other)
-    for p in kv_far:
-        if p // Y and p % Y:
-            greet((z + p // Y) % Z * Y + (y + p % Y) % Y, tp)
-
     copies = {
         n: pltpu.make_async_copy(r[n], r[n + "_v"], r["lsem"].at[i]) for i, n in enumerate(args)
     }
+    copies["tok"].start()
+
+    peers = {(dz, 0, 0, 0) for dz in range(Z)} | {(dz, dy, 0, 0) for dz in range(Z) for dy in range(Y)}
+    peers |= {(near[n], dy, dx, 0) for n in {0} | set(AG_DIRECT) | set(RS_DIRECT) for dy in range(Y) for dx in range(X)}
+    peers |= {(0, 0, dx, dc) for dx in range(X) for dc in range(C)}
+    peers -= {(0, 0, 0, 0)}
+    barrier = pltpu.get_barrier_semaphore()
+    for dz, dy, dx, dc in sorted(peers, key=lambda o: (-hops(o[0], Z) - hops(o[1], Y) - hops(o[2], X), o)):
+        to = ((z + dz) % Z * Y + (y + dy) % Y, (x + dx) % X * C + (c + dc) % C)
+        pl.semaphore_signal(barrier, inc=1, device_id=to, device_id_type=MESH)
+
     for n in args:
-        copies[n].start()
-
-    for k in "12":
-        r["xall" + k][:, :, other] = jnp.zeros((Z, YX, ROWS, B), bf16)
-    r["hid"][...] = jnp.zeros_like(r["hid"])
-    r["tr"][...] = jnp.zeros_like(r["tr"])
-    r["wmisc"][...] = jnp.zeros_like(r["wmisc"])
+        if n != "tok":
+            copies[n].start()
+
     copies["tok"].wait()
-    pl.semaphore_wait(barrier, (Z - 1) + (YX - 1) + X + (Z - 1) * (Y - 1))
-
-    def plane(send):
-        for p in plane_far:
+    r["xall1"][yx, c, 0] = r["tok_v"][...]
+    pl.semaphore_wait(barrier, len(peers))
+
+    def clear():
+        for k in "12":
+            r["xall" + k][:, other] = jnp.zeros((YX, Z, ROWS, B), bf16)
+        r["hid"][...] = jnp.zeros_like(r["hid"])
+        r["tr"][...] = jnp.zeros_like(r["tr"])
+        r["wmisc"][...] = jnp.zeros_like(r["wmisc"])
+
+    def plane(send, dz=0):
+        for p in plane_far if dz == 0 else [*plane_far, 0]:
             yt, xt = (y + p // X) % Y, (x + p % X) % X
-            send(p, yt * X + xt, z * Y + yt, xt * C + c)
+            send(p, yt * X + xt, (z + dz) % Z * Y + yt, xt * C + c)
 
     def swap_weights(k):
         for i, n in enumerate(("wg", "wu", "wd")):
@@ -134,41 +142,65 @@
             tr[48:92, :] = r["wds" + k][:, cols].astype(f32)
             dt[zz] = jnp.transpose(tr[...]).astype(bf16).reshape(YX, C, ROWS, 128)
 
-    def mlp(k, after_sends, after_z, after_scatter):
-        xall, ebuf, erec, sbuf, prow, zbuf, zrec = (
-            r[n + k] for n in ("xall", "ebuf", "erec", "sbuf", "prow", "zbuf", "zrec")
+    def mlp(k, after_sends, after_z, before_last):
+        xall, ebuf, erec, sbuf, prow, drow, first, zbuf, zrec = (
+            r[n + k] for n in ("xall", "ebuf", "erec", "sbuf", "prow", "drow", "first", "zbuf", "zrec")
         )
         az, ap, ex, rp, rz, saz, sap, srp, srz = (
             r[n + k] for n in ("az", "ap", "ex", "rp", "rz", "saz", "sap", "srp", "srz")
         )
         hid = r["hid"]
 
-        def spread(i):
+        def at_z(n):
+            return (z + near[n]) % Z * Y + y
+
+        def blocks(n, first):
+            return prow.at[pl.ds(first, YX - first), pl.ds(0, n)]
+
+        def spread(group):
+            part = xall.at[yx, c, pl.ds(group[0], len(group))]
+
             def send(p, target, kv_to, tp_to):
-                remote(xall.at[i, yx, c], xall.at[i, yx, c], sap.at[i], ap.at[i], kv_to, tp_to).start()
+                remote(part, part, sap.at[group[0]], ap.at[group[0]], kv_to, tp_to).start()
 
             plane(send)
 
-        for dz in far:
-            if dz:
-                kv_to = (z + dz) % Z * Y + y
-                remote(xall.at[0, yx, c], xall.at[dz, yx, c], saz.at[dz], az.at[dz], kv_to, tp).start()
-        spread(0)
+        def spread_direct(n):
+            mine, there = xall.at[yx, c, 0], xall.at[yx, c, n]
+
+            def send(p, target, kv_to, tp_to):
+                remote(mine, there, sap.at[n], ap.at[n], kv_to, tp_to).start()
+
+            plane(send, near[n])
+
+        for n in range(Z)[::-1]:
+            if n and n not in AG_DIRECT and n not in AG_LATE:
+                remote(xall.at[yx, c, 0], xall.at[yx, c, n], saz.at[n], az.at[n], at_z(n), tp).start()
+        spread(AG_GROUPS[0])
+        for n in AG_DIRECT:
+            spread_direct(n)
         after_sends()
-        for i in near[1:]:
-            wait_for(xall.at[i, yx, c], az.at[i])
-            spread(i)
+        for group in AG_GROUPS[1:]:
+            for n in group:
+                wait_for(xall.at[yx, c, n], az.at[n])
+            spread(group)
         after_z()
 
         squares = jnp.zeros((8, B), f32)
         sums = jnp.zeros((192, B), f32)
-        for i in near:
-            wait_for(prow.at[0, pl.ds(1, YX - 1)], ap.at[i])
-            sums += jnp.dot(
-                r["wp" + k][(z - i + Z) % Z], xall[i].reshape(G, B), preferred_element_type=f32
-            )
-            wide = xall[i, :, c].astype(f32)
-            squares += jnp.sum((wide * wide).reshape(YX * ROWS // 8, 8, B), axis=0)
+        for group in AG_ORDER:
+            if group[0] in AG_LATE:
+                wait_for(xall.at[:, c, group[0]], az.at[group[0]])
+            else:
+                wait_for(blocks(len(group), 0 if group[0] in AG_DIRECT else 1), ap.at[group[0]])
+            if group[0] == 0:
+                for n in AG_LATE:
+                    remote(xall.at[:, c, 0], xall.at[:, c, n], saz.at[n], az.at[n], at_z(n), tp).start()
+            for n in group:
+                rows = xall[:, :, n].reshape(G, B)
+                sums += jnp.dot(r["wp" + k][(z - near[n] + Z) % Z], rows, preferred_element_type=f32)
+                wide = xall[:, c, n].astype(f32)
+                squares += jnp.sum((wide * wide).reshape(YX * ROWS // 8, 8, B), axis=0)
         ebuf[0:192] = sums
         ebuf[192:200] = squares
         both = remote(ebuf, erec, ex.at[0], ex.at[1], kv, x * C + other)
@@ -181,43 +213,79 @@
             gate, up = total[0:48], total[48:96]
             hid[mine // 2 : mine // 2 + 48] = (gate / (1.0 + jnp.exp(-gate)) * up).astype(bf16)
 
-        for i in far:
-            weight = r["dt" + k][(z + i) % Z, :, c].reshape(YX * ROWS, 128)
-            terms = jnp.dot(weight, hid[...], preferred_element_type=f32)
-            sbuf[i] = terms.reshape(YX, ROWS, B).astype(bf16)
-
-            def send(p, target, kv_to, tp_to):
-                remote(sbuf.at[i, target], prow.at[i, p], srp.at[i], rp.at[i], kv_to, tp_to).start()
-
-            plane(send)
-        after_scatter()
-
-        total = None
-        for i in far:
-            wait_for(prow.at[i, pl.ds(1, YX - 1)], rp.at[i])
-            total = jnp.sum(prow[i, 1:YX].astype(f32), axis=0) + sbuf[i, yx].astype(f32)
-            if i:
-                zbuf[i] = total
-                kv_to = (z + i) % Z * Y + y
-                remote(zbuf.at[i], zrec.at[i], srz.at[i], rz.at[i], kv_to, tp).start()
-        for i in near[1:]:
-            wait_for(zrec.at[i], rz.at[i])
-            total = total + zrec[i]
+        for group in RS_ORDER:
+            for n in group:
+                weight = r["dt" + k][(z + near[n]) % Z, :, c].reshape(YX * ROWS, 128)
+                terms = jnp.dot(weight, hid[...], preferred_element_type=f32).reshape(YX, ROWS, B)
+                if n == 0:
+                    before_last()
+                    for at, m in enumerate(RS_FIRST):
+                        wait_for(first.at[at], rz.at[m])
+                        terms += first[at].astype(f32)
+                sbuf[:, n] = terms.astype(bf16)
+            n = group[0]
+            if n in RS_FIRST:
+                at = RS_FIRST.index(n)
+                remote(sbuf.at[:, n], first.at[at], srz.at[n], rz.at[n], at_z(n), tp).start()
+                continue
+            if n in RS_DIRECT:
+                at = RS_DIRECT.index(n)
+
+                def send(p, target, kv_to, tp_to):
+                    remote(sbuf.at[target, n], drow.at[at, p], srp.at[n], rp.at[n], kv_to, tp_to).start()
+
+                plane(send, near[n])
+            else:
+                some = pl.ds(n, len(group))
+
+                def send(p, target, kv_to, tp_to):
+                    remote(
+                        sbuf.at[target, some], prow.at[p, some], srp.at[n], rp.at[n], kv_to, tp_to
+                    ).start()
+
+                plane(send)
+
+        total = jnp.zeros((ROWS, B), f32)
+        for group in RS_ORDER:
+            if group[0] in RS_DIRECT or group[0] in RS_FIRST:
+                continue
+            wait_for(blocks(len(group), 1), rp.at[group[0]])
+            for n in group[::-1]:
+                part = jnp.sum(prow[1:YX, n].astype(f32), axis=0) + sbuf[yx, n].astype(f32)
+                if n:
+                    zbuf[n] = part
+                    remote(zbuf.at[n], zrec.at[n], srz.at[n], rz.at[n], at_z(n), tp).start()
+                else:
+                    total += part
+        for n in RS_DIRECT:
+            wait_for(drow.at[RS_DIRECT.index(n)], rp.at[n])
+            total += jnp.sum(drow[RS_DIRECT.index(n)].astype(f32), axis=0)
+        for n in range(1, Z):
+            if n not in RS_DIRECT and n not in RS_FIRST:
+                wait_for(zrec.at[n], rz.at[n])
+                total += zrec[n]
 
         def drain():
             both.wait_send()
             for i, n in enumerate(("wgs", "wus", "wds")):
                 wait_for(r[n + k], r["ssw" + k].at[i])
-            for i in range(Z):
-                if i:
-                    wait_for(xall.at[0, yx, c], saz.at[i])
-                    wait_for(zbuf.at[i], srz.at[i])
-                wait_for(prow.at[i, pl.ds(1, YX - 1)], sap.at[i])
-                wait_for(prow.at[i, pl.ds(1, YX - 1)], srp.at[i])
+            for n in range(1, Z):
+                if n in AG_LATE:
+                    wait_for(xall.at[:, c, n], saz.at[n])
+                elif n not in AG_DIRECT:
+                    wait_for(xall.at[yx, c, n], saz.at[n])
+                if n in RS_FIRST:
+                    wait_for(sbuf.at[:, n], srz.at[n])
+                elif n not in RS_DIRECT:
+                    wait_for(zbuf.at[n], srz.at[n])
+            for order, direct, sem in ((AG_ORDER, AG_DIRECT, sap), (RS_ORDER, RS_DIRECT, srp)):
+                for group in order:
+                    if group[0] in (AG_LATE if sem is sap else RS_FIRST):
+                        continue
+                    wait_for(blocks(len(group), 0 if group[0] in direct else 1), sem.at[group[0]])
 
         return 0.5 * total, drain
 
-    r["xall1"][0, yx, c] = r["tok_v"][...]
 
     def prep_mix():
         for n in ("gm", "wq", "wk", "wv", "wo", "wi", "wf", "fb", "hg", "wm", "mem", "stab"):
@@ -232,13 +300,19 @@
         prep_up("1")
         prep_down("1")
 
-    def prep_second():
+    def start_first():
+        swap_weights("1")
+        clear()
+
+    def before_mix():
         swap_weights("2")
         prep_mix()
+
+    def prep_second():
         prep_up("2")
         prep_down("2")
 
-    half, drain1 = mlp("1", lambda: swap_weights("1"), prep_first, prep_second)
+    half, drain1 = mlp("1", start_first, prep_first, before_mix)
     first = (r["tok_v"][...].astype(f32) + half).astype(bf16)
 
     fbuf = r["fbuf"]
@@ -280,24 +354,35 @@
     def seqs(kv_of):
         return kv_of // 2, kv_of % 2
 
-    for i in far:
-        zt = (z + i) % Z
-        for dy in range(1, Y):
-            a, b = seqs(zt * Y + (y + dy) % Y)
-            remote(
-                sm.at[a, b], yrec.at[i, dy], r["smy"].at[i], r["my"].at[i], z * Y + (y + dy) % Y, tp
-            ).start()
-    mine = None
-    for i in far:
-        wait_for(yrec.at[i, pl.ds(1, Y - 1)], r["my"].at[i])
-        a, b = seqs((z + i) % Z * Y + y)
-        mine = jnp.sum(yrec[i, 1:Y].astype(f32), axis=0) + sm[a, b].astype(f32)
-        if i:
-            zb[i] = mine.astype(bf16)
-            remote(zb.at[i], zr.at[i], r["smz"].at[i], r["mz"].at[i], (z + i) % Z * Y + y, tp).start()
-    for i in near[1:]:
-        wait_for(zr.at[i], r["mz"].at[i])
-        mine = mine + zr[i].astype(f32)
+    def to_kv(n, dy):
+        return (z + near[n]) % Z * Y + (y + dy) % Y
+
+    for n in range(Z)[::-1]:
+        for dy in range(Y)[::-1]:
+            if dy or n in KS_DIRECT:
+                to = to_kv(n, dy)
+                through = to if n in KS_DIRECT else to_kv(0, dy)
+                a, b = seqs(to)
+                remote(sm.at[a, b], yrec.at[n, dy], r["smy"].at[n], r["my"].at[n], through, tp).start()
+    mine = jnp.zeros((32, 128), f32)
+    for n in range(Z)[::-1]:
+        if n in KS_DIRECT:
+            continue
+        wait_for(yrec.at[n, pl.ds(1, Y - 1)], r["my"].at[n])
+        a, b = seqs(to_kv(n, 0))
+        part = jnp.sum(yrec[n, 1:Y].astype(f32), axis=0) + sm[a, b].astype(f32)
+        if n:
+            zb[n] = part.astype(bf16)
+            remote(zb.at[n], zr.at[n], r["smz"].at[n], r["mz"].at[n], to_kv(n, 0), tp).start()
+        else:
+            mine += part
+    for n in range(1, Z):
+        if n in KS_DIRECT:
+            wait_for(yrec.at[n], r["my"].at[n])
+            mine += jnp.sum(yrec[n].astype(f32), axis=0)
+        else:
+            wait_for(zr.at[n], r["mz"].at[n])
+            mine += zr[n].astype(f32)
 
     lane8 = lax.broadcasted_iota(jnp.int32, (8, 128), 1)
     row8 = lax.broadcasted_iota(jnp.int32, (8, 128), 0)
@@ -348,13 +433,14 @@
     gated = readout * lax.rsqrt(mean + EPS) * head_gain / (1.0 + jnp.exp(-outgate))
 
     mm = r["mm"]
-    mm[kv] = rounded(gated)
+    mm[kv] = gated.astype(bf16)
     for p in kv_far:
         kv_to = (z + p // Y) % Z * Y + (y + p % Y) % Y
         remote(mm.at[kv], mm.at[kv], r["ns"].at[0], r["ns"].at[1], kv_to, tp).start()
+    prep_second()
     others = mm.at[pl.ds(0, kv_size - 1)]
     wait_for(others, r["ns"].at[1])
-    pairs = mm[...].reshape(B // 8, 2, 8, 128)
+    pairs = mm[...].astype(f32).reshape(B // 8, 2, 8, 128)
     a, b = pairs[:, 0], pairs[:, 1]
     left = jnp.where(low, a, pltpu.roll(b, 4, 1)).reshape(B, 128).astype(bf16)
     right = jnp.where(low, pltpu.roll(a, 4, 1), b).reshape(B, 128).astype(bf16)
@@ -373,7 +459,7 @@
     branch = r["of32"][tp] + jnp.sum(r["orec"][1:TP].astype(f32), axis=0)
     after_mix = (first.astype(f32) + branch).astype(bf16)
 
-    r["xall2"][0, yx, c] = after_mix
+    r["xall2"][yx, c, 0] = after_mix
     half, drain2 = mlp("2", nothing, nothing, nothing)
     r["out_o"][...] = (after_mix.astype(f32) + half).astype(bf16)
     drain1()
@@ -381,10 +467,32 @@
     wait_for(fbuf.at[pl.ds(1, TP - 1)], r["fs"].at[0])
     wait_for(r["orec"].at[pl.ds(1, TP - 1)], r["os"].at[0])
     wait_for(others, r["ns"].at[0])
-    for i in range(Z):
-        wait_for(yrec.at[i, pl.ds(1, Y - 1)], r["smy"].at[i])
-        if i:
-            wait_for(zb.at[i], r["smz"].at[i])
+    for n in range(Z):
+        if n in KS_DIRECT:
+            wait_for(yrec.at[n], r["smy"].at[n])
+        else:
+            wait_for(yrec.at[n, pl.ds(1, Y - 1)], r["smy"].at[n])
+            if n:
+                wait_for(zb.at[n], r["smz"].at[n])
+
+
+def finish(*refs):
+    source, target, held, sems = refs[0:3], refs[3:6], refs[6:9], refs[9]
+    parts = [(1, i) for i in range(SEQ)] + [(0, None), (2, None)]
+
+    def at(refs, k):
+        which, i = parts[k]
+        return refs[which] if i is None else refs[which].at[i]
+
+    ins = [pltpu.make_async_copy(at(source, k), at(held, k), sems.at[0, k]) for k in range(6)]
+    outs = [pltpu.make_async_copy(at(held, k), at(target, k), sems.at[1, k]) for k in range(6)]
+    for copy in ins:
+        copy.start()
+    for copy, out in zip(ins, outs):
+        copy.wait()
+        out.start()
+    for out in outs:
+        out.wait()
 
 
 def on_device(kv_size, tp_size, *args):
@@ -416,11 +524,13 @@
         raw,
         pltpu.VMEM((Z, 192, G), bf16),
         pltpu.VMEM((Z, YX, C, ROWS, 128), bf16),
-        pltpu.VMEM((Z, YX, C, ROWS, B), bf16),
+        pltpu.VMEM((YX, C, Z, ROWS, B), bf16),
         pltpu.VMEM((200, B), f32),
         pltpu.VMEM((200, B), f32),
-        pltpu.VMEM((Z, YX, ROWS, B), bf16),
-        pltpu.VMEM((Z, YX, ROWS, B), bf16),
+        pltpu.VMEM((YX, Z, ROWS, B), bf16),
+        pltpu.VMEM((YX, Z, ROWS, B), bf16),
+        pltpu.VMEM((max(1, len(RS_DIRECT)), YX, ROWS, B), bf16),
+        pltpu.VMEM((max(1, len(RS_FIRST)), YX, ROWS, B), bf16),
         pltpu.VMEM((Z, ROWS, B), f32),
         pltpu.VMEM((Z, ROWS, B), f32),
         DMA((3,)),
@@ -449,7 +559,7 @@
         pltpu.VMEM((Z, Y, 32, 128), bf16),
         pltpu.VMEM((Z, 32, 128), bf16),
         pltpu.VMEM((Z, 32, 128), bf16),
-        pltpu.VMEM((kv_size, 8, 128), f32),
+        pltpu.VMEM((kv_size, 8, 128), bf16),
         pltpu.VMEM((TP, ROWS, B), bf16),
         pltpu.VMEM((TP, ROWS, B), f32),
         pltpu.VMEM((TP, ROWS, B), bf16),
@@ -473,6 +583,15 @@
         ),
         name="decode_step",
     )(*operands)
+    out, memory_next, stabilizer_next = pl.pallas_call(
+        finish,
+        out_shape=out_shapes,
+        in_specs=[pl.BlockSpec(memory_space=pl.ANY)] * 3,
+        out_specs=[pl.BlockSpec(memory_space=pl.ANY)] * 3,
+        scratch_shapes=[*(pltpu.VMEM(o.shape, o.dtype) for o in out_shapes), DMA((2, 6))],
+        compiler_params=pltpu.CompilerParams(vmem_limit_bytes=60 * 1024 * 1024),
+        name="finish",
+    )(out, memory_next, stabilizer_next)
     return out.T, memory_next, stabilizer_next.T
 
 

time: 87.2 us -> 82.5 us (0.946)
  local copies, waits for them, and re-layouts: 3.64 us -> 0 us
  Pallas kernels: 82.1 us -> 81 us
    unnamed x7 -> x0, local copies, waits for them, and re-layouts: 3.64 us -> none
    pallas_call x1, Pallas kernels: 82.1 us -> 79.2 us  [on_device(): pl.pallas_call(functools.partial(kernel, kv_size, tp_size), out_shape=out...]
    pallas_call x0 -> x1, Pallas kernels: none -> 1.86 us  [on_device(): pl.pallas_call(finish, out_shape=out_shapes, in_specs=[pl.BlockSpec(memor...]
where the time goes in v1:
time: 82.5 us; the launch traced here: 82.3 us
  Pallas kernels  81 us (98%)
  between operations  1.29 us (2%)
    pallas_call x1, Pallas kernels, on_device(): pl.pallas_call(functools.partial(kernel, kv_size, tp_size), out_shape=out...  79.2 us
    pallas_call x1, Pallas kernels, on_device(): pl.pallas_call(finish, out_shape=out_shapes, in_specs=[pl.BlockSpec(memor...  1.86 us

profile of v1, /device:TPU:1, one launch (start us, length us, event | category | flops | bytes accessed | tf_op | source)
XLA Modules:
  0.0 82.3 jit_solution(906767364416065111)
XLA Ops:
  1.3 79.2 %decode_step.1 = (bf16[16,128]{1,0:T(8,128)(2,1)}, f32[4,1,128,256]{3,2,1,0:T(8,128)}, f32[1,4]{1,0:T(1,128)}) custom-call(bf16[16,128]{1,0:T(8,128)(2,1)} %bitcast.16, bf16[4096]{0:T(1024)(128)(2,1)} %refs_1_.1, bf16[44,4096]{1,0:T(8,128)(2,1)} %bitcast.12, bf16[44,4096]{1,0:T(8,128)(2,1)} %bitcast.13, bf16[44,4096]{1,0:T(8,128)(2,1)} %refs_4_.1, ...), custom_call_target="tpu_custom_call" | custom-call | tf_op jit(solution)/shard_map/decode_step/pallas_call | solution.py:575
  80.5 1.9 %finish.1 = (bf16[16,128]{1,0:T(8,128)(2,1)}, f32[4,1,128,256]{3,2,1,0:T(8,128)}, f32[1,4]{1,0:T(1,128)}) custom-call(bf16[16,128]{1,0:T(8,128)(2,1)} %get-tuple-element.9.refs_0_, f32[4,1,128,256]{3,2,1,0:T(8,128)} %get-tuple-element.10.refs_1_, f32[1,4]{1,0:T(1,128)} %get-tuple-element.11.refs_2_), custom_call_target="tpu_custom_call" | custom-call | tf_op jit(solution)/shard_map/finish/pallas_call | solution.py:586
